TPU v7x, 512 devices: a whole 4x8x8 slice. The times are simulated.
512 devices in a mesh: sp: 64 (over z, y), tp: 8 (over x, core).
Axes of the slice: x: 4, y: 8, z: 8, core: 2. Of those that a mesh axis runs over, the one named last changes fastest.
Arguments:
- tokens: bfloat16 [16384, 2048], P('sp', 'tp'), may hold values from -24 to 24
- value_weight: bfloat16 [2, 2048, 2048], P(None, 'sp', 'tp'), may hold values from -0.125 to 0.125
- outer_weight: bfloat16 [2, 2048, 2048], P(None, 'sp', 'tp'), may hold values from -0.125 to 0.125
- inner_weight: bfloat16 [2, 2048, 2048], P(None, 'sp', 'tp'), may hold values from -0.125 to 0.125
- conv_taps: float32 [2, 3, 2048], P(None, None, 'tp'), may hold values from -3.5 to 3.5
- output_weight: bfloat16 [2, 2048, 2048], P(None, 'tp', 'sp'), may hold values from -2 to 2
- norm_gain: float32 [2, 2048], P(None, 'tp'), may hold values from 0.1 to 1.9
- norm_bias: float32 [2, 2048], P(None, 'tp'), may hold values from -3 to 3
Outputs:
- mixed_out: bfloat16 [16384, 2048], P('sp', 'tp')
All inputs are finite; a program needn't handle non-finite values.
Results may differ from a plain program's by a relative error of at most 0.03.
Values may be sent and summed in bfloat16 or wider, within the bound.
No kernel may reach another device: no remote copies, remote signals or barrier semaphores. Data moves between devices by JAX's collectives and lax.ppermute only.
A program may use at most 64 MiB of HBM per device.

v0:
```python
import jax
import jax.numpy as jnp
from jax import lax
from jax.sharding import Mesh, PartitionSpec as P

D = 2048
LAYERS = 2
TP = ("x", "core")
SP = ("z", "y")
HALO = 16
IN_UP, OUT_UP = (2.0**18, 2.0**14)


def bf(x):
    return x.astype(jnp.bfloat16)


def f32(x):
    return x.astype(jnp.float32)


def rounded(x):
    return lax.reduce_precision(x, exponent_bits=8, mantissa_bits=7)


def thirds(x):
    a = rounded(x)
    b = rounded(x - a)
    c = rounded(x - a - b)
    return jnp.stack([bf(a), bf(b), bf(c)])


def packed(value, outer, inner, out, layer):
    return jnp.concatenate([value[layer], outer[layer], inner[layer], out[layer].T], axis=1)


def norm(pre, gain, bias):
    mean = jnp.mean(pre, axis=-1, keepdims=True)
    cent = pre - mean
    var = jnp.mean(cent * cent, axis=-1, keepdims=True)
    return bf(cent * lax.rsqrt(var + 1e-05) * gain + bias)


def gated_rows(x, w_in, down, taps, first, head):
    width = w_in.shape[1] // 3
    acc = jnp.dot(x, w_in, preferred_element_type=jnp.float32) * down
    u, outer, inner = (f32(bf(acc[:, i * width : (i + 1) * width])) for i in range(3))
    z = inner * u
    row = lax.broadcasted_iota(jnp.int32, z.shape, 0)
    z = jnp.where(jnp.logical_and(first, row < head), 0.0, z)
    conv = taps[2] * z[2:] + taps[1] * z[1:-1] + taps[0] * z[:-2]
    return bf(outer[2:] * conv)


def out_product(g, w_out_t, down):
    return (
        lax.dot_general(g, w_out_t, (((1,), (1,)), ((), ())), preferred_element_type=jnp.float32)
        * down
    )


def pair_sum(main, extra, w_out_t, down, core):
    blocks = main.reshape(4, 2, 32, -1)
    mine = jnp.where(core == 0, blocks[:, 0], blocks[:, 1]).reshape(128, -1)
    other = jnp.where(core == 0, blocks[:, 1], blocks[:, 0]).reshape(128, -1)
    if extra is not None:
        mine = jnp.concatenate([mine, extra], axis=0)
        other = jnp.concatenate([other, extra], axis=0)
    sent = bf(out_product(other, w_out_t, down))
    got = lax.ppermute(sent, "core", [(0, 1), (1, 0)])
    return out_product(mine, w_out_t, down) + f32(got)


def shards(tokens, value, outer, inner, taps, out, gain, bias):
    alpha = (2.0 * LAYERS) ** 0.25
    core = lax.axis_index("core")
    sp = lax.axis_index(SP)
    tp = lax.axis_index(TP)
    first = sp == 0
    late = lax.all_gather(packed(value, outer, inner, out, 1), SP, axis=0, tiled=True)
    halo = lax.ppermute(tokens[-HALO:], SP, [(i, i + 1) for i in range(63)])
    params = jnp.concatenate([gain, bias], axis=0)
    parts = thirds(params).reshape(12, 256)
    parts = jnp.concatenate([parts, jnp.zeros((4, 256), jnp.bfloat16)], axis=0)
    mine = jnp.concatenate([halo, tokens, parts], axis=0)
    everyone = lax.all_to_all(jnp.broadcast_to(mine[None], (8, *mine.shape)), TP, 0, 0, tiled=True)
    scale = jnp.where(jnp.arange(1024) < 768, IN_UP, OUT_UP)
    early = (f32(packed(value, outer, inner, out, 0)) * scale).astype(jnp.float16)
    early = lax.all_gather(early, SP, axis=0, tiled=True)
    early = bf(early)
    whole = jnp.moveaxis(everyone, 0, 1).reshape(288, D)
    table = f32(whole[272:284]).reshape(3, 4, D)
    table = table[0] + table[1] + table[2]
    x0 = whole[:272]
    g = gated_rows(x0, early[:, :768], 1.0 / IN_UP, taps[0], first, HALO)
    branch = pair_sum(g[HALO - 2 :], g[HALO - 10 : HALO - 2], early[:, 768:], 1.0 / OUT_UP, core)
    main = bf(branch[:128]).reshape(4, 32, D)
    extra = bf(branch[134:136]).reshape(32, 128)
    send = jnp.concatenate([main, jnp.broadcast_to(extra[None], (4, 32, 128))], axis=2)
    got = jnp.sum(f32(lax.all_to_all(send, "x", 0, 0, tiled=True)), axis=0)
    own = lax.dynamic_slice_in_dim(x0, HALO + 32 * tp, 32, axis=0)
    pre = jnp.concatenate(
        [
            alpha * f32(own) + got[:, :D],
            alpha * f32(x0[HALO - 2 : HALO]) + got[:, D:].reshape(2, D),
        ],
        axis=0,
    )
    state = norm(pre, table[0], table[2])
    own = state[:32]
    every = lax.all_gather(own.astype(jnp.float16), TP, axis=0, tiled=True)
    x1 = jnp.concatenate([jnp.zeros((6, D), jnp.bfloat16), state[32:], bf(every)], axis=0)
    g = gated_rows(x1, late[:, :768], 1.0, taps[1], first, 8)
    branch = pair_sum(g[6:], None, late[:, 768:], 1.0, core)
    got = lax.all_to_all(bf(branch).reshape(4, 32, D), "x", 0, 0, tiled=True)
    pre = alpha * f32(own) + jnp.sum(f32(got), axis=0)
    state = norm(pre, table[1], table[3])
    back = jnp.moveaxis(state.reshape(32, 8, 256), 1, 0)
    return lax.all_to_all(back, TP, 0, 0, tiled=True).reshape(256, 256)


def solution(mesh):
    mesh = Mesh(mesh.devices.reshape(8, 8, 4, 2), ("z", "y", "x", "core"))
    in_specs = (
        P(SP, TP),
        P(None, SP, TP),
        P(None, SP, TP),
        P(None, SP, TP),
        P(None, None, TP),
        P(None, TP, SP),
        P(None, TP),
        P(None, TP),
    )
    return jax.shard_map(shards, mesh=mesh, in_specs=in_specs, out_specs=P(SP, TP), check_vma=False)
```

profile of v0, /device:TPU:1, one launch (start us, length us, event | category | flops | bytes accessed | tf_op | source)
XLA Modules:
  0.0 170.9 jit_solution(12494518444327532426)
XLA Ops:
  6.5 0.7 slice_bitcast_fusion.8
  7.3 0.7 slice_bitcast_fusion.5
  8.0 0.8 slice_bitcast_fusion.6
  8.8 0.6 pad_maximum_fusion.6
  9.4 0.7 slice.214
  10.1 4.0 %collective-permute-start = (bf16[16,256]{1,0:T(8,128)(2,1)S(1)}, bf16[16,256]{1,0:T(8,128)(2,1)S(1)}, u32[]{:S(2)}, u32[]{:S(2)}) collective-permute-start(bf16[16,256]{1,0:T(8,128)(2,1)S(1)} %slice.214), channel_id=1, source_target_pairs={{0,8},{8,16},{16,24},{24,32},{32,40},{40,48},{48,56},{56,64},{64,7... | collective-permute-start | bytes 24584 | tf_op jit(solution)/shard_map/ppermute | solution.py:81
  14.2 0.7 reduce-precision_convert_fusion.1
  15.0 1.0 maximum_maximum_fusion
  16.1 1.2 broadcast_in_dim.41
  17.2 8.0 %all-to-all-start = ((bf16[8,288,256]{2,1,0:T(8,128)(2,1)}), bf16[8,288,256]{2,1,0:T(8,128)(2,1)S(1)}, u32[]{:S(2)}, u32[]{:S(2)}) async-start(bf16[8,288,256]{2,1,0:T(8,128)(2,1)} %broadcast_in_dim.41), calls=%async_computation | async-start | bytes 2359296 | tf_op jit(solution)/shard_map/all_to_all | solution.py:86
  25.3 56.9 %all-gather.5 = f16[2048,1024]{1,0:T(8,128)(2,1)S(1)} all-gather(f16[32,1024]{1,0:T(8,128)(2,1)S(1)} %multiply_convert_fusion), channel_id=1, replica_groups=mesh['z'=8,'y'=8,'x'=4,'core'=2] {'z','y'}, dimensions={0}, use_global_device_ids=true | all-gather | bytes 4259840 | tf_op jit(solution)/shard_map/all_gather | solution.py:89
  82.2 3.2 %convert_element_type.120 = bf16[2048,1024]{1,0:T(8,128)(2,1)} convert(f16[2048,1024]{1,0:T(8,128)(2,1)S(1)} %all-gather.5) | non-fusion elementwise | flops 2097152 | bytes 8388608 | tf_op jit(solution)/shard_map/convert_element_type | solution.py:15
  85.6 2.0 %copy-done = bf16[2048,1024]{1,0:T(8,128)(2,1)S(1)} copy-done((bf16[2048,1024]{1,0:T(8,128)(2,1)S(1)}, bf16[2048,1024]{1,0:T(8,128)(2,1)}, u32[]{:S(2)}) %copy-start) | copy-done | bytes 4194328
  87.6 1.1 fusion.8
  89.0 0.5 fusion.4
  89.5 11.2 %collective-permute-start.1 = (bf16[136,2048]{1,0:T(8,128)(2,1)S(1)}, bf16[136,2048]{1,0:T(8,128)(2,1)S(1)}, u32[]{:S(2)}, u32[]{:S(2)}) collective-permute-start(bf16[136,2048]{1,0:T(8,128)(2,1)S(1)} %fusion.4), channel_id=1, source_target_pairs={{0,1},{1,0},{2,3},{3,2},{4,5},{5,4},{6,7},{7,6},{8,9},{9,8},{10,11... | collective-permute-start | bytes 1671176 | tf_op jit(solution)/shard_map/ppermute | solution.py:70
  100.8 1.5 collective-permute-done.1
  102.3 0.5 add_convert_fusion
  102.9 0.9 pad_maximum_fusion
  103.8 4.7 %all-to-all-start.1 = ((bf16[4,32,2176]{2,1,0:T(8,128)(2,1)}), bf16[4,32,2176]{2,1,0:T(8,128)(2,1)S(1)}, u32[]{:S(2)}, u32[]{:S(2)}) async-start(bf16[4,32,2176]{2,1,0:T(8,128)(2,1)} %pad_maximum_fusion), calls=%async_computation.1 | async-start | bytes 1114112 | tf_op jit(solution)/shard_map/all_to_all | solution.py:100
  108.6 9.2 %all-to-all-done.1 = bf16[4,32,2176]{2,1,0:T(8,128)(2,1)S(1)} async-done(((bf16[4,32,2176]{2,1,0:T(8,128)(2,1)}), bf16[4,32,2176]{2,1,0:T(8,128)(2,1)S(1)}, u32[]{:S(2)}, u32[]{:S(2)}) %all-to-all-start.1) | async-done | bytes 557088 | tf_op jit(solution)/shard_map/all_to_all | solution.py:100
  118.1 0.2 multiply_reduce_fusion
  118.5 15.2 %all-gather.6 = f16[256,2048]{1,0:T(8,128)(2,1)S(1)} all-gather(f16[32,2048]{1,0:T(8,128)(2,1)S(1)} %slice_convert_fusion), channel_id=1, replica_groups=mesh['z'=8,'y'=8,'x'=4,'core'=2] {'x','core'}, dimensions={0}, use_global_device_ids=true | all-gather | bytes 1179648 | tf_op jit(solution)/shard_map/all_gather | solution.py:111
  134.0 3.1 %fusion.11 = bf16[264,768]{1,0:T(8,128)(2,1)S(1)} fusion(bf16[2048,1024]{1,0:T(8,128)(2,1)} %all-gather.4.cloned.1.call-done, bf16[256,2048]{1,0:T(8,128)(2,1)S(1)} %convert_element_type.132, bf16[2,2048]{1,0:T(2,128)(2,1)S(1)} %slice.296, bf16[264]{0:T(512)(128)(2,1)S(1)} %pad.4.clone), kind=kOutput, calls=%fused_computation.10 | convolution fusion | flops 833918976 | bytes 4608528 | tf_op jit(solution)/shard_map/dot_general | solution.py:46
  137.5 0.5 convolution_convert_fusion
  138.0 2.1 %collective-permute-start.2 = (bf16[128,2048]{1,0:T(8,128)(2,1)S(1)}, bf16[128,2048]{1,0:T(8,128)(2,1)S(1)}, u32[]{:S(2)}, u32[]{:S(2)}) collective-permute-start(bf16[128,2048]{1,0:T(8,128)(2,1)S(1)} %convolution_convert_fusion), channel_id=1, source_target_pairs={{0,1},{1,0},{2,3},{3,2},{4,5},{5,4},{6,7},{7,6},{8,9},{9,8},{10,11... | collective-permute-start | bytes 1572872 | tf_op jit(solution)/shard_map/ppermute | solution.py:70
  140.1 1.7 %collective-permute-done.2 = bf16[128,2048]{1,0:T(8,128)(2,1)S(1)} collective-permute-done((bf16[128,2048]{1,0:T(8,128)(2,1)S(1)}, bf16[128,2048]{1,0:T(8,128)(2,1)S(1)}, u32[]{:S(2)}, u32[]{:S(2)}) %collective-permute-start.2) | collective-permute-done | bytes 524320 | tf_op jit(solution)/shard_map/ppermute | solution.py:70
  141.8 0.5 add_convert_fusion.1
  142.3 11.7 %all_to_all.20 = bf16[4,32,2048]{2,1,0:T(8,128)(2,1)S(1)} all-to-all(bf16[4,32,2048]{2,1,0:T(8,128)(2,1)S(1)} %bitcast.57), channel_id=1, replica_groups=mesh['z'=8,'y'=8,'x'=4,'core'=2] {'x'}, dimensions={0} | all-to-all | bytes 1048576 | tf_op jit(solution)/shard_map/all_to_all | solution.py:115
  154.2 0.2 multiply_reduce_fusion.1
  154.7 8.8 %all_to_all.21 = bf16[8,32,256]{2,1,0:T(8,128)(2,1)S(1)} all-to-all(bf16[8,32,256]{2,1,0:T(8,128)(2,1)S(1)} %copy.11), channel_id=1, replica_groups=mesh['z'=8,'y'=8,'x'=4,'core'=2] {'x','core'}, dimensions={0} | all-to-all | bytes 262144 | tf_op jit(solution)/shard_map/all_to_all | solution.py:119
  163.4 0.7 copy.15
  (60 shorter events, 2.3 us)
Async XLA Ops:
  6.5 127.5 %all-gather.4.cloned.1.call-start = ((), (), s32[]{:S(2)}) async-start(), calls=%async_computation.4 | async-start | bytes 4259840 | tf_op jit(solution)/shard_map/all_gather | solution.py:80
  10.1 4.9 %collective-permute-start = (bf16[16,256]{1,0:T(8,128)(2,1)S(1)}, bf16[16,256]{1,0:T(8,128)(2,1)S(1)}, u32[]{:S(2)}, u32[]{:S(2)}) collective-permute-start(bf16[16,256]{1,0:T(8,128)(2,1)S(1)} %slice.214), channel_id=1, source_target_pairs={{0,8},{8,16},{16,24},{24,32},{32,40},{40,48},{48,56},{56,64},{64,7... | collective-permute-start | bytes 24584 | tf_op jit(solution)/shard_map/ppermute | solution.py:81
  17.2 68.2 %all-to-all-start = ((bf16[8,288,256]{2,1,0:T(8,128)(2,1)}), bf16[8,288,256]{2,1,0:T(8,128)(2,1)S(1)}, u32[]{:S(2)}, u32[]{:S(2)}) async-start(bf16[8,288,256]{2,1,0:T(8,128)(2,1)} %broadcast_in_dim.41), calls=%async_computation | async-start | bytes 2359296 | tf_op jit(solution)/shard_map/all_to_all | solution.py:86
  82.1 3.2 %copy-start.2 = (f32[2,3,256]{2,0,1:T(2,128)S(1)}, f32[2,3,256]{2,0,1:T(2,128)}, u32[]{:S(2)}) copy-start(f32[2,3,256]{2,0,1:T(2,128)} %param.12) | copy-start | bytes 18436
  85.4 2.2 %copy-start = (bf16[2048,1024]{1,0:T(8,128)(2,1)S(1)}, bf16[2048,1024]{1,0:T(8,128)(2,1)}, u32[]{:S(2)}) copy-start(bf16[2048,1024]{1,0:T(8,128)(2,1)} %convert_element_type.120) | copy-start | bytes 12582916
  89.5 12.8 %collective-permute-start.1 = (bf16[136,2048]{1,0:T(8,128)(2,1)S(1)}, bf16[136,2048]{1,0:T(8,128)(2,1)S(1)}, u32[]{:S(2)}, u32[]{:S(2)}) collective-permute-start(bf16[136,2048]{1,0:T(8,128)(2,1)S(1)} %fusion.4), channel_id=1, source_target_pairs={{0,1},{1,0},{2,3},{3,2},{4,5},{5,4},{6,7},{7,6},{8,9},{9,8},{10,11... | collective-permute-start | bytes 1671176 | tf_op jit(solution)/shard_map/ppermute | solution.py:70
  103.8 14.0 %all-to-all-start.1 = ((bf16[4,32,2176]{2,1,0:T(8,128)(2,1)}), bf16[4,32,2176]{2,1,0:T(8,128)(2,1)S(1)}, u32[]{:S(2)}, u32[]{:S(2)}) async-start(bf16[4,32,2176]{2,1,0:T(8,128)(2,1)} %pad_maximum_fusion), calls=%async_computation.1 | async-start | bytes 1114112 | tf_op jit(solution)/shard_map/all_to_all | solution.py:100
  134.0 3.5 %copy-start.1 = (bf16[2048,1024]{1,0:T(8,128)(2,1)S(1)}, bf16[2048,1024]{1,0:T(8,128)(2,1)}, u32[]{:S(2)}) copy-start(bf16[2048,1024]{1,0:T(8,128)(2,1)} %all-gather.4.cloned.1.call-done) | copy-start | bytes 12582916
  138.0 3.8 %collective-permute-start.2 = (bf16[128,2048]{1,0:T(8,128)(2,1)S(1)}, bf16[128,2048]{1,0:T(8,128)(2,1)S(1)}, u32[]{:S(2)}, u32[]{:S(2)}) collective-permute-start(bf16[128,2048]{1,0:T(8,128)(2,1)S(1)} %convolution_convert_fusion), channel_id=1, source_target_pairs={{0,1},{1,0},{2,3},{3,2},{4,5},{5,4},{6,7},{7,6},{8,9},{9,8},{10,11... | collective-permute-start | bytes 1572872 | tf_op jit(solution)/shard_map/ppermute | solution.py:70
Sparse Core Ops, SparseCore 0:
  10.4 93.0 all-gather.3
where the time goes:
time: 172 us; the launch traced here: 171 us
  blocking collectives  92.5 us (54%)
  starting transfers between devices  30.1 us (18%)
  between operations  13.8 us (8%)
  waiting for transfers between devices  12.5 us (7%)
  other arithmetic  8.44 us (5%)
  local copies, waits for them, and re-layouts  7.43 us (4%)
  matrix products  6.15 us (4%)
    all_gather x1, blocking collectives, shards(): early = lax.all_gather(early, SP, axis=0, tiled=True)  56.9 us
    all_gather x1, blocking collectives, shards(): every = lax.all_gather(own.astype(jnp.float16), TP, axis=0, tiled=True)  15.2 us
    ppermute x2, starting transfers between devices, pair_sum(): got = lax.ppermute(sent, 'core', [(0, 1), (1, 0)])  13.3 us
    all_to_all x1, blocking collectives, shards(): got = lax.all_to_all(bf(branch).reshape(4, 32, D), 'x', 0, 0, tiled=True)  11.7 us
    all_to_all x1, waiting for transfers between devices, shards(): got = jnp.sum(f32(lax.all_to_all(send, 'x', 0, 0, tiled=True)), axis=0)  9.22 us
    all_to_all x1, blocking collectives, shards(): return lax.all_to_all(back, TP, 0, 0, tiled=True).reshape(256, 256)  8.78 us
    all_to_all x1, starting transfers between devices, shards(): lax.all_to_all(jnp.broadcast_to(mine[None], (8, *mine.shape)), TP, 0, 0,...  8.04 us
    all_to_all x1, starting transfers between devices, shards(): got = jnp.sum(f32(lax.all_to_all(send, 'x', 0, 0, tiled=True)), axis=0)  4.74 us
  transfers between devices with their start and end apart: 6, of which 3 were waited for; matrix products, arithmetic and copies ran while one was open for 7% of the time, Pallas kernels for 0%

commit v1 on v0

--- a/solution.py
+++ b/solution.py
@@ -2,6 +2,7 @@
 import jax.numpy as jnp
 from jax import lax
 from jax.sharding import Mesh, PartitionSpec as P
+from jax.lax import all_to_all, axis_size
 
 D = 2048
 LAYERS = 2
@@ -86,7 +87,10 @@
     everyone = lax.all_to_all(jnp.broadcast_to(mine[None], (8, *mine.shape)), TP, 0, 0, tiled=True)
     scale = jnp.where(jnp.arange(1024) < 768, IN_UP, OUT_UP)
     early = (f32(packed(value, outer, inner, out, 0)) * scale).astype(jnp.float16)
-    early = lax.all_gather(early, SP, axis=0, tiled=True)
+    find_links = lambda page: jnp.concatenate(
+        all_to_all(jnp.stack([page] * axis_size(SP)), SP, 0, 0), axis=0
+    )
+    early = find_links(early)
     early = bf(early)
     whole = jnp.moveaxis(everyone, 0, 1).reshape(288, D)
     table = f32(whole[272:284]).reshape(3, 4, D)

time: 172 us -> 267 us (1.55)
  waiting for transfers between devices: 12.5 us -> 149 us
  blocking collectives: 92.5 us -> 37.2 us
  starting transfers between devices: 30.1 us -> 45.3 us
    all_to_all x0 -> x1, waiting for transfers between devices: none -> 101 us  [shards(): all_to_all(jnp.stack([page] * axis_size(SP)), SP, 0, 0)]
    all_gather x1 -> x0, blocking collectives: 56.9 us -> none  [shards(): early = lax.all_gather(early, SP, axis=0, tiled=True)]
    all_gather x1, waiting for transfers between devices: 0.02 us -> 19.4 us  [shards(): lax.all_gather(packed(value, outer, inner, out, 1), SP, axis=0, tiled=True)]
    all_to_all x1, waiting for transfers between devices: 0.01 us -> 16.3 us  [shards(): lax.all_to_all(jnp.broadcast_to(mine[None], (8, *mine.shape)), TP, 0, 0,...]
    all_to_all x0 -> x1, starting transfers between devices: none -> 16.3 us  [shards(): all_to_all(jnp.stack([page] * axis_size(SP)), SP, 0, 0)]
  transfers between devices with their start and end apart: 6 -> 7, of which waited for: 3 -> 6; matrix products, arithmetic and copies ran while one was open for 7% -> 4% of each run, Pallas kernels for 0% -> 0%
where the time goes in v1:
time: 267 us; the launch traced here: 266 us
  waiting for transfers between devices  149 us (56%)
  starting transfers between devices  45.3 us (17%)
  blocking collectives  37.2 us (14%)
  between operations  13.9 us (5%)
  other arithmetic  8.61 us (3%)
  matrix products  6.18 us (2%)
  local copies, waits for them, and re-layouts  5.62 us (2%)
    all_to_all x1, waiting for transfers between devices, shards(): all_to_all(jnp.stack([page] * axis_size(SP)), SP, 0, 0)  101 us
    all_gather x1, waiting for transfers between devices, shards(): lax.all_gather(packed(value, outer, inner, out, 1), SP, axis=0, tiled=True)  19.4 us
    all_to_all x1, waiting for transfers between devices, shards(): lax.all_to_all(jnp.broadcast_to(mine[None], (8, *mine.shape)), TP, 0, 0,...  16.3 us
    all_to_all x1, starting transfers between devices, shards(): all_to_all(jnp.stack([page] * axis_size(SP)), SP, 0, 0)  16.3 us
    all_gather x1, blocking collectives, shards(): every = lax.all_gather(own.astype(jnp.float16), TP, axis=0, tiled=True)  15.2 us
    all_to_all x1, blocking collectives, shards(): got = lax.all_to_all(bf(branch).reshape(4, 32, D), 'x', 0, 0, tiled=True)  12.5 us
    ppermute x2, starting transfers between devices, pair_sum(): got = lax.ppermute(sent, 'core', [(0, 1), (1, 0)])  11.1 us
    all_to_all x1, blocking collectives, shards(): return lax.all_to_all(back, TP, 0, 0, tiled=True).reshape(256, 256)  9.42 us
  transfers between devices with their start and end apart: 7, of which 6 were waited for; matrix products, arithmetic and copies ran while one was open for 4% of the time, Pallas kernels for 0%

profile of v1, /device:TPU:1, one launch (start us, length us, event | category | flops | bytes accessed | tf_op | source)
XLA Modules:
  0.0 266.0 jit_solution(17641822992023955704)
XLA Ops:
  6.5 0.7 slice.214
  7.2 4.0 %collective-permute-start = (bf16[16,256]{1,0:T(8,128)(2,1)S(1)}, bf16[16,256]{1,0:T(8,128)(2,1)S(1)}, u32[]{:S(2)}, u32[]{:S(2)}) collective-permute-start(bf16[16,256]{1,0:T(8,128)(2,1)S(1)} %slice.214), channel_id=1, source_target_pairs={{0,8},{8,16},{16,24},{24,32},{32,40},{40,48},{48,56},{56,64},{64,7... | collective-permute-start | bytes 24584 | tf_op jit(solution)/shard_map/ppermute | solution.py:82
  11.2 0.7 reduce-precision_convert_fusion.1
  12.1 1.0 maximum_maximum_fusion
  13.1 1.1 broadcast_in_dim.41
  14.2 8.2 %all-to-all-start = ((bf16[8,288,256]{2,1,0:T(8,128)(2,1)}), bf16[8,288,256]{2,1,0:T(8,128)(2,1)S(1)}, u32[]{:S(2)}, u32[]{:S(2)}) async-start(bf16[8,288,256]{2,1,0:T(8,128)(2,1)} %broadcast_in_dim.41), calls=%async_computation | async-start | bytes 2359296 | tf_op jit(solution)/shard_map/all_to_all | solution.py:87
  22.6 16.3 %all-to-all-done = bf16[8,288,256]{2,1,0:T(8,128)(2,1)S(1)} async-done(((bf16[8,288,256]{2,1,0:T(8,128)(2,1)}), bf16[8,288,256]{2,1,0:T(8,128)(2,1)S(1)}, u32[]{:S(2)}, u32[]{:S(2)}) %all-to-all-start) | async-done | bytes 1179680 | tf_op jit(solution)/shard_map/all_to_all | solution.py:87
  38.8 2.5 stack.5
  41.4 16.3 %all-to-all-start.1 = ((f16[64,32,1024]{2,1,0:T(8,128)(2,1)}), f16[64,32,1024]{2,1,0:T(8,128)(2,1)}, u32[]{:S(2)}, u32[]{:S(2)}) async-start(f16[64,32,1024]{2,1,0:T(8,128)(2,1)} %stack.5), calls=%async_computation.1 | async-start | bytes 8388608 | tf_op jit(solution)/shard_map/all_to_all | solution.py:91
  57.7 0.6 pad_maximum_fusion.6
  58.7 101.4 %all-to-all-done.1 = f16[64,32,1024]{2,1,0:T(8,128)(2,1)} async-done(((f16[64,32,1024]{2,1,0:T(8,128)(2,1)}), f16[64,32,1024]{2,1,0:T(8,128)(2,1)}, u32[]{:S(2)}, u32[]{:S(2)}) %all-to-all-start.1) | async-done | bytes 4194336 | tf_op jit(solution)/shard_map/all_to_all | solution.py:91
  160.0 3.4 %convert_element_type.127 = bf16[64,32,1024]{2,1,0:T(8,128)(2,1)S(1)} convert(f16[64,32,1024]{2,1,0:T(8,128)(2,1)} %all-to-all-done.1) | non-fusion elementwise | flops 2097152 | bytes 8388608 | tf_op jit(solution)/shard_map/convert_element_type | solution.py:16
  163.4 1.1 fusion.8
  164.8 0.5 fusion.4
  165.3 4.4 %collective-permute-start.1 = (bf16[136,2048]{1,0:T(8,128)(2,1)S(1)}, bf16[136,2048]{1,0:T(8,128)(2,1)S(1)}, u32[]{:S(2)}, u32[]{:S(2)}) collective-permute-start(bf16[136,2048]{1,0:T(8,128)(2,1)S(1)} %fusion.4), channel_id=1, source_target_pairs={{0,1},{1,0},{2,3},{3,2},{4,5},{5,4},{6,7},{7,6},{8,9},{9,8},{10,11... | collective-permute-start | bytes 1671176 | tf_op jit(solution)/shard_map/ppermute | solution.py:71
  169.8 1.5 collective-permute-done.1
  171.3 0.5 add_convert_fusion
  171.9 0.9 pad_maximum_fusion
  172.7 5.6 %all-to-all-start.2 = ((bf16[4,32,2176]{2,1,0:T(8,128)(2,1)}), bf16[4,32,2176]{2,1,0:T(8,128)(2,1)S(1)}, u32[]{:S(2)}, u32[]{:S(2)}) async-start(bf16[4,32,2176]{2,1,0:T(8,128)(2,1)} %pad_maximum_fusion), calls=%async_computation.2 | async-start | bytes 1114112 | tf_op jit(solution)/shard_map/all_to_all | solution.py:104
  178.4 9.2 %all-to-all-done.2 = bf16[4,32,2176]{2,1,0:T(8,128)(2,1)S(1)} async-done(((bf16[4,32,2176]{2,1,0:T(8,128)(2,1)}), bf16[4,32,2176]{2,1,0:T(8,128)(2,1)S(1)}, u32[]{:S(2)}, u32[]{:S(2)}) %all-to-all-start.2) | async-done | bytes 557088 | tf_op jit(solution)/shard_map/all_to_all | solution.py:104
  187.9 0.2 multiply_reduce_fusion
  188.4 15.2 %all-gather.4 = f16[256,2048]{1,0:T(8,128)(2,1)S(1)} all-gather(f16[32,2048]{1,0:T(8,128)(2,1)S(1)} %slice_convert_fusion), channel_id=1, replica_groups=mesh['z'=8,'y'=8,'x'=4,'core'=2] {'x','core'}, dimensions={0}, use_global_device_ids=true | all-gather | bytes 1179648 | tf_op jit(solution)/shard_map/all_gather | solution.py:115
  203.8 19.4 %all-gather.3.cloned.1.call-done = bf16[2048,1024]{1,0:T(8,128)(2,1)} async-done(((bf16[32,1024]{1,0:T(8,128)(2,1)}), bf16[2048,1024]{1,0:T(8,128)(2,1)}) %all-gather.3.cloned.1.call-update) | async-done | bytes 4194320 | tf_op jit(solution)/shard_map/all_gather | solution.py:81
  223.1 3.1 %fusion.11 = bf16[264,768]{1,0:T(8,128)(2,1)S(1)} fusion(bf16[2048,1024]{1,0:T(8,128)(2,1)} %all-gather.3.cloned.1.call-done, bf16[256,2048]{1,0:T(8,128)(2,1)S(1)} %convert_element_type.140, bf16[2,2048]{1,0:T(2,128)(2,1)S(1)} %slice.296, bf16[264]{0:T(512)(128)(2,1)S(1)} %pad.4.clone), kind=kOutput, calls=%fused_computation.10 | convolution fusion | flops 833918976 | bytes 4608528 | tf_op jit(solution)/shard_map/dot_general | solution.py:47
  226.7 0.5 convolution_convert_fusion
  227.2 6.7 %collective-permute-start.2 = (bf16[128,2048]{1,0:T(8,128)(2,1)S(1)}, bf16[128,2048]{1,0:T(8,128)(2,1)S(1)}, u32[]{:S(2)}, u32[]{:S(2)}) collective-permute-start(bf16[128,2048]{1,0:T(8,128)(2,1)S(1)} %convolution_convert_fusion), channel_id=1, source_target_pairs={{0,1},{1,0},{2,3},{3,2},{4,5},{5,4},{6,7},{7,6},{8,9},{9,8},{10,11... | collective-permute-start | bytes 1572872 | tf_op jit(solution)/shard_map/ppermute | solution.py:71
  233.9 1.5 collective-permute-done.2
  235.4 0.5 add_convert_fusion.1
  235.9 12.5 %all_to_all.25 = bf16[4,32,2048]{2,1,0:T(8,128)(2,1)S(1)} all-to-all(bf16[4,32,2048]{2,1,0:T(8,128)(2,1)S(1)} %bitcast.61), channel_id=1, replica_groups=mesh['z'=8,'y'=8,'x'=4,'core'=2] {'x'}, dimensions={0} | all-to-all | bytes 1048576 | tf_op jit(solution)/shard_map/all_to_all | solution.py:119
  248.7 0.2 multiply_reduce_fusion.1
  249.1 9.4 %all_to_all.26 = bf16[8,32,256]{2,1,0:T(8,128)(2,1)S(1)} all-to-all(bf16[8,32,256]{2,1,0:T(8,128)(2,1)S(1)} %copy.11), channel_id=1, replica_groups=mesh['z'=8,'y'=8,'x'=4,'core'=2] {'x','core'}, dimensions={0} | all-to-all | bytes 262144 | tf_op jit(solution)/shard_map/all_to_all | solution.py:123
  258.5 0.7 copy.15
  (68 shorter events, 2.4 us)
Async XLA Ops:
  7.2 4.9 %collective-permute-start = (bf16[16,256]{1,0:T(8,128)(2,1)S(1)}, bf16[16,256]{1,0:T(8,128)(2,1)S(1)}, u32[]{:S(2)}, u32[]{:S(2)}) collective-permute-start(bf16[16,256]{1,0:T(8,128)(2,1)S(1)} %slice.214), channel_id=1, source_target_pairs={{0,8},{8,16},{16,24},{24,32},{32,40},{40,48},{48,56},{56,64},{64,7... | collective-permute-start | bytes 24584 | tf_op jit(solution)/shard_map/ppermute | solution.py:82
  14.2 8.2 %copy-start.1 = (bf16[2,32,256]{2,1,0:T(8,128)(2,1)S(1)}, bf16[2,32,256]{2,1,0:T(8,128)(2,1)}, u32[]{:S(2)}) copy-start(bf16[2,32,256]{2,1,0:T(8,128)(2,1)} %param.9) | copy-start | bytes 98308
  14.2 8.3 %copy-start.2 = (bf16[2,256,32]{1,2,0:T(8,128)(2,1)S(1)}, bf16[2,256,32]{1,2,0:T(8,128)(2,1)}, u32[]{:S(2)}) copy-start(bf16[2,256,32]{1,2,0:T(8,128)(2,1)} %param.13) | copy-start | bytes 98308
  14.2 8.3 %copy-start.3 = (bf16[2,32,256]{2,1,0:T(8,128)(2,1)S(1)}, bf16[2,32,256]{2,1,0:T(8,128)(2,1)}, u32[]{:S(2)}) copy-start(bf16[2,32,256]{2,1,0:T(8,128)(2,1)} %param.11) | copy-start | bytes 98308
  14.2 8.3 %copy-start.4 = (bf16[2,32,256]{2,1,0:T(8,128)(2,1)S(1)}, bf16[2,32,256]{2,1,0:T(8,128)(2,1)}, u32[]{:S(2)}) copy-start(bf16[2,32,256]{2,1,0:T(8,128)(2,1)} %param.10) | copy-start | bytes 98308
  14.2 24.6 %all-to-all-start = ((bf16[8,288,256]{2,1,0:T(8,128)(2,1)}), bf16[8,288,256]{2,1,0:T(8,128)(2,1)S(1)}, u32[]{:S(2)}, u32[]{:S(2)}) async-start(bf16[8,288,256]{2,1,0:T(8,128)(2,1)} %broadcast_in_dim.41), calls=%async_computation | async-start | bytes 2359296 | tf_op jit(solution)/shard_map/all_to_all | solution.py:87
  41.4 17.1 %copy-start.5 = (f32[2,3,256]{2,0,1:T(2,128)S(1)}, f32[2,3,256]{2,0,1:T(2,128)}, u32[]{:S(2)}) copy-start(f32[2,3,256]{2,0,1:T(2,128)} %param.12) | copy-start | bytes 18436
  41.4 118.7 %all-to-all-start.1 = ((f16[64,32,1024]{2,1,0:T(8,128)(2,1)}), f16[64,32,1024]{2,1,0:T(8,128)(2,1)}, u32[]{:S(2)}, u32[]{:S(2)}) async-start(f16[64,32,1024]{2,1,0:T(8,128)(2,1)} %stack.5), calls=%async_computation.1 | async-start | bytes 8388608 | tf_op jit(solution)/shard_map/all_to_all | solution.py:91
  57.6 165.5 %all-gather.3.cloned.1.call-start = ((), (), s32[]{:S(2)}) async-start(), calls=%async_computation.5 | async-start | bytes 4259840 | tf_op jit(solution)/shard_map/all_gather | solution.py:81
  165.3 6.0 %collective-permute-start.1 = (bf16[136,2048]{1,0:T(8,128)(2,1)S(1)}, bf16[136,2048]{1,0:T(8,128)(2,1)S(1)}, u32[]{:S(2)}, u32[]{:S(2)}) collective-permute-start(bf16[136,2048]{1,0:T(8,128)(2,1)S(1)} %fusion.4), channel_id=1, source_target_pairs={{0,1},{1,0},{2,3},{3,2},{4,5},{5,4},{6,7},{7,6},{8,9},{9,8},{10,11... | collective-permute-start | bytes 1671176 | tf_op jit(solution)/shard_map/ppermute | solution.py:71
  172.7 14.9 %all-to-all-start.2 = ((bf16[4,32,2176]{2,1,0:T(8,128)(2,1)}), bf16[4,32,2176]{2,1,0:T(8,128)(2,1)S(1)}, u32[]{:S(2)}, u32[]{:S(2)}) async-start(bf16[4,32,2176]{2,1,0:T(8,128)(2,1)} %pad_maximum_fusion), calls=%async_computation.2 | async-start | bytes 1114112 | tf_op jit(solution)/shard_map/all_to_all | solution.py:104
  223.1 3.5 %copy-start = (bf16[2048,1024]{1,0:T(8,128)(2,1)S(1)}, bf16[2048,1024]{1,0:T(8,128)(2,1)}, u32[]{:S(2)}) copy-start(bf16[2048,1024]{1,0:T(8,128)(2,1)} %all-gather.3.cloned.1.call-done) | copy-start | bytes 12582916
  227.2 8.2 %collective-permute-start.2 = (bf16[128,2048]{1,0:T(8,128)(2,1)S(1)}, bf16[128,2048]{1,0:T(8,128)(2,1)S(1)}, u32[]{:S(2)}, u32[]{:S(2)}) collective-permute-start(bf16[128,2048]{1,0:T(8,128)(2,1)S(1)} %convolution_convert_fusion), channel_id=1, source_target_pairs={{0,1},{1,0},{2,3},{3,2},{4,5},{5,4},{6,7},{7,6},{8,9},{9,8},{10,11... | collective-permute-start | bytes 1572872 | tf_op jit(solution)/shard_map/ppermute | solution.py:71
Sparse Core Ops, SparseCore 0:
  61.5 161.5 all-gather.2
